TPU v7x, 32 devices: a whole 2x2x4 slice. The times are simulated.
32 devices in a mesh: sp: 16 (over z, y, x), tp: 2 (over core).
Axes of the slice: x: 2, y: 2, z: 4, core: 2. Of those that a mesh axis runs over, the one named last changes fastest.
Arguments:
- residual_in: bfloat16 [4096, 2048], P(('sp', 'tp')), may hold values from -6 to 6
- query_lean: bfloat16 [4096, 8, 96], P('sp', 'tp'), may hold values from -60 to 60
- query_broad: bfloat16 [4096, 8, 160], P('sp', 'tp'), may hold values from -60 to 60
- latent: bfloat16 [4096, 256], P('sp'), may hold values from -6 to 6
- rope_key: bfloat16 [4096, 32], P('sp'), may hold values from -8 to 8
- latent_gain: float32 [256], replicated, may hold values from 0.1 to 1.9
- key_up_lean: bfloat16 [256, 8, 64], P(None, 'tp'), may hold values from -0.375 to 0.375
- key_up_broad: bfloat16 [256, 8, 128], P(None, 'tp'), may hold values from -0.375 to 0.375
- value_up_lean: bfloat16 [256, 8, 64], P(None, 'tp'), may hold values from -0.375 to 0.375
- value_up_broad: bfloat16 [256, 8, 128], P(None, 'tp'), may hold values from -0.375 to 0.375
- out_lean: bfloat16 [8, 64, 2048], P('tp'), may hold values from -0.15625 to 0.15625
- out_broad: bfloat16 [8, 128, 2048], P('tp'), may hold values from -0.15625 to 0.15625
- attn_gain: float32 [2048], replicated, may hold values from 0.1 to 1.9
- mlp_gain: float32 [2048], replicated, may hold values from 0.1 to 1.9
- gate_weight: bfloat16 [2048, 2816], P('sp', 'tp'), may hold values from -0.125 to 0.125
- up_weight: bfloat16 [2048, 2816], P('sp', 'tp'), may hold values from -0.125 to 0.125
- down_weight: bfloat16 [2816, 2048], P('tp', 'sp'), may hold values from -0.109375 to 0.109375
Outputs:
- layer_out: bfloat16 [4096, 2048], P(('sp', 'tp'))
All inputs are finite; a program needn't handle non-finite values.
Results may differ from a plain program's by a relative error of at most 0.015.
Values may be sent and summed in bfloat16 or wider, within the bound.
A program may use at most 128 MiB of HBM per device.

v0:
```python
import math
import jax
import jax.numpy as jnp
from jax import lax
from jax.sharding import PartitionSpec as P

THETA = 10000.0
EPS = 1e-06
NEGATIVE = -1e30


def rotate(values, positions):
    width = values.shape[-1]
    half = width // 2
    freqs = THETA ** (-2.0 * jnp.arange(half, dtype=jnp.float32) / width)
    angle = positions.astype(jnp.float32)[:, None] * freqs[None, :]
    cosine = jnp.cos(angle)
    sine = jnp.sin(angle)
    if values.ndim == 3:
        cosine = cosine[:, None, :]
        sine = sine[:, None, :]
    first = values[..., :half]
    second = values[..., half:]
    return jnp.concatenate(
        [first * cosine - second * sine, first * sine + second * cosine], axis=-1
    )


def normalize(values, gain):
    return values * lax.rsqrt(jnp.mean(values * values, axis=-1, keepdims=True) + EPS) * gain


def block_keys(weights, latent_rows):
    projected = []
    for key_up, value_up in weights:
        keys = jnp.einsum(
            "kr,rhd->khd", latent_rows, key_up, preferred_element_type=jnp.float32
        ).astype(jnp.bfloat16)
        values = jnp.einsum(
            "kr,rhd->khd", latent_rows, value_up, preferred_element_type=jnp.float32
        ).astype(jnp.bfloat16)
        projected.append((keys, values))
    return projected


def attend(carry, queries, projected, rotated_rows, key_pos, query_pos):
    updated = []
    visible = key_pos[None, :] <= query_pos[:, None]
    for state, query, pair in zip(carry, queries, projected):
        query_nope, query_rot, scale = query
        keys, values = pair
        peak, total, accum = state
        scores = (
            jnp.einsum("qhd,khd->hqk", query_nope, keys, preferred_element_type=jnp.float32)
            + jnp.einsum("qhr,kr->hqk", query_rot, rotated_rows, preferred_element_type=jnp.float32)
        ) * scale
        scores = jnp.where(visible[None], scores, NEGATIVE)
        new_peak = jnp.maximum(peak, jnp.max(scores, axis=-1))
        weights = jnp.where(visible[None], jnp.exp(scores - new_peak[..., None]), 0.0)
        factor = jnp.exp(peak - new_peak)
        total = total * factor + jnp.sum(weights, axis=-1)
        accum = accum * factor[..., None] + jnp.einsum(
            "hqk,khv->hqv", weights.astype(jnp.bfloat16), values, preferred_element_type=jnp.float32
        )
        updated.append((new_peak, total, accum))
    return tuple(updated)


def fold_piece(carry, latent_piece, rotated_piece, piece_pos, weights, segments):
    count = latent_piece.shape[0]
    block = math.gcd(count, 1024)
    last_all = segments[0][1][-1]

    def one_block(index, state):
        lat_rows = lax.dynamic_slice_in_dim(latent_piece, index * block, block, 0)
        rot_rows = lax.dynamic_slice_in_dim(rotated_piece, index * block, block, 0)
        pos_rows = lax.dynamic_slice_in_dim(piece_pos, index * block, block, 0)
        first_key = jnp.min(pos_rows)

        def work(inner):
            projected = block_keys(weights, lat_rows)
            results = []
            for inner_seg, segment in zip(inner, segments):
                queries, seg_pos = segment
                results.append(
                    lax.cond(
                        first_key <= seg_pos[-1],
                        lambda held, queries=queries, seg_pos=seg_pos: attend(
                            held, queries, projected, rot_rows, pos_rows, seg_pos
                        ),
                        lambda held: held,
                        inner_seg,
                    )
                )
            return tuple(results)

        return lax.cond(first_key <= last_all, work, lambda inner: inner, state)

    return lax.fori_loop(0, count // block, one_block, carry)


def shards(
    residual_in,
    query_lean,
    query_broad,
    latent,
    rope_key,
    latent_gain,
    key_up_lean,
    key_up_broad,
    value_up_lean,
    value_up_broad,
    out_lean,
    out_broad,
    attn_gain,
    mlp_gain,
    gate_weight,
    up_weight,
    down_weight,
):
    tokens_here = query_lean.shape[0]
    n_tp = lax.axis_size("tp")
    share = tokens_here // n_tp
    sp_index = lax.axis_index("sp")
    first = sp_index * tokens_here
    query_pos = first + jnp.arange(tokens_here, dtype=jnp.int32)
    rope_width = rope_key.shape[1]
    weights = ((key_up_lean, value_up_lean), (key_up_broad, value_up_broad))
    segment_rows = (query_lean, query_broad, query_pos)
    segments = []
    initial = []
    lean_rows, broad_rows, seg_pos = segment_rows
    queries = []
    states = []
    for query, value_up in ((lean_rows, value_up_lean), (broad_rows, value_up_broad)):
        nope = query.shape[2] - rope_width
        query_rot = rotate(query[:, :, nope:].astype(jnp.float32), seg_pos).astype(jnp.bfloat16)
        queries.append((query[:, :, :nope], query_rot, query.shape[2] ** (-0.5)))
        heads = query.shape[1]
        rows = query.shape[0]
        states.append(
            (
                jnp.full((heads, rows), NEGATIVE, jnp.float32),
                jnp.zeros((heads, rows), jnp.float32),
                jnp.zeros((heads, rows, value_up.shape[2]), jnp.float32),
            )
        )
    segments.append((tuple(queries), seg_pos))
    initial.append(tuple(states))
    segments = tuple(segments)
    initial = tuple(initial)
    sent_latent = normalize(latent.astype(jnp.float32), latent_gain).astype(jnp.bfloat16)
    sent_rot = rotate(rope_key.astype(jnp.float32), query_pos).astype(jnp.bfloat16)
    pieces = (
        lax.all_gather(sent_latent, "sp", axis=0, tiled=True),
        lax.all_gather(sent_rot, "sp", axis=0, tiled=True),
    )
    piece_pos = jnp.arange(pieces[0].shape[0], dtype=jnp.int32)
    folded = fold_piece(initial, pieces[0], pieces[1], piece_pos, weights, segments)
    results = [
        [(accum / total[..., None]).astype(jnp.bfloat16) for peak, total, accum in seg_state]
        for seg_state in folded
    ]
    attended = results[0]
    term = jnp.zeros((share * lax.axis_size("tp"), out_lean.shape[2]), jnp.float32)
    for rows_all, weight in ((attended[0], out_lean), (attended[1], out_broad)):
        rows = rows_all
        term = term + jnp.einsum("hqv,hvd->qd", rows, weight, preferred_element_type=jnp.float32)
    head_sum = lax.psum_scatter(
        term.astype(jnp.bfloat16), "tp", scatter_dimension=0, tiled=True
    ).astype(jnp.float32)
    branch = normalize(head_sum, attn_gain)
    kept = (residual_in.astype(jnp.float32) + branch).astype(jnp.bfloat16)
    normed = normalize(kept.astype(jnp.float32), mlp_gain).astype(jnp.bfloat16)
    whole_normed = lax.all_gather(normed, "tp", axis=0, tiled=True)
    gate_whole, up_whole, down_whole = (
        lax.all_gather(gate_weight, "sp", axis=0, tiled=True),
        lax.all_gather(up_weight, "sp", axis=0, tiled=True),
        lax.all_gather(down_weight, "sp", axis=1, tiled=True),
    )
    gate = jnp.dot(whole_normed, gate_whole, preferred_element_type=jnp.float32)
    up = jnp.dot(whole_normed, up_whole, preferred_element_type=jnp.float32)
    hidden = (jax.nn.silu(gate) * up).astype(jnp.bfloat16)
    rows = hidden
    channel_sum = lax.psum_scatter(
        jnp.dot(rows, down_whole, preferred_element_type=jnp.float32).astype(jnp.bfloat16),
        "tp",
        scatter_dimension=0,
        tiled=True,
    ).astype(jnp.float32)
    return (kept.astype(jnp.float32) + 0.5 * channel_sum).astype(jnp.bfloat16)


def solution(mesh):
    in_specs = (
        P(("sp", "tp"), None),
        P("sp", "tp", None),
        P("sp", "tp", None),
        P("sp", None),
        P("sp", None),
        P(),
        P(None, "tp", None),
        P(None, "tp", None),
        P(None, "tp", None),
        P(None, "tp", None),
        P("tp", None, None),
        P("tp", None, None),
        P(),
        P(),
        P("sp", "tp"),
        P("sp", "tp"),
        P("tp", "sp"),
    )
    out_specs = P(("sp", "tp"), None)
    return jax.shard_map(shards, mesh=mesh, in_specs=in_specs, out_specs=out_specs, check_vma=False)
```

profile of v0, /device:TPU:0, one launch (start us, length us, event | category | flops | bytes accessed | tf_op | source)
XLA Modules:
  0.0 533.8 jit_solution(12831282787911574293)
XLA Ops:
  6.5 1.2 fusion.57
  7.7 1.7 fusion.59
  9.5 0.7 convert_element_type.107
  10.2 0.6 slice.38
  10.8 1.0 slice.45
  11.8 0.9 copy.25
  12.7 1.0 copy.21
  13.7 1.7 copy.22
  15.4 0.9 slice.39
  16.5 0.9 slice_convert_fusion
  17.4 0.7 pad_maximum_fusion
  18.1 0.6 pad_maximum_fusion.1
  18.7 47.5 %all_gather.19 = bf16[4096,32]{0,1:T(8,128)(2,1)} all-gather(bf16[256,32]{0,1:T(8,128)(2,1)S(1)} %pad_maximum_fusion.2), channel_id=1, replica_groups=mesh['sp'=16,'tp'=2] {'sp'}, dimensions={0}, use_global_device_ids=true | all-gather | bytes 278528 | tf_op jit(solution)/shard_map/all_gather | solution.py:156
  66.2 8.1 %all-gather.6.cloned.1.call-done = bf16[4096,256]{1,0:T(8,128)(2,1)} async-done(((bf16[256,256]{1,0:T(8,128)(2,1)}), bf16[4096,256]{1,0:T(8,128)(2,1)}) %all-gather.6.cloned.1.call-update) | async-done | bytes 2097168 | tf_op jit(solution)/shard_map/all_gather | solution.py:155
  74.2 0.6 iota.15
  74.8 0.8 broadcast_in_dim.44
  75.7 0.7 broadcast_in_dim.43
  76.4 0.6 broadcast.136.clone
  77.0 38.2 %while.24 = (s32[]{:T(128)}, f32[4,256]{1,0:T(4,128)S(1)}, f32[4,256]{1,0:T(4,128)S(1)}, f32[4,256,64]{1,2,0:T(8,128)}, f32[4,256]{1,0:T(4,128)S(1)}, /*index=5*...) while((s32[]{:T(128)}, f32[4,256]{1,0:T(4,128)S(1)}, ...), condition=%wide.region_11.12_spmd.clone, body=%wide.region_1.11_spmd.clone.sunk | while | flops 1768035584 | bytes 76572688 | solution.py:99
  77.0 1.4 fusion.91
  78.4 0.6 iota.27
  80.2 25.2 %conditional.4 = ((f32[4,256]{1,0:T(4,128)S(1)}, f32[4,256]{1,0:T(4,128)S(1)}, f32[4,256,64]{1,2,0:T(8,128)}, f32[4,256]{1,0:T(4,128)S(1)}, f32[4,256]{1,0:T(4,128)}, /*index=5*/f32[4,256,128]{2,1,0:T(8,128)})) conditional(s32[]{:T(128)} %convert_element_type.184, (f32[4,256]{1,0:T(4,128)S(1)}, f32[4,256]{1,0:T(4,128)S(1)}, f32[4,256,64]{1,2,0:T(8,128)}, ...), branch_computations={%region_3.0_spmd, %region_4.10_spmd} | conditional | flops 1768034560 | bytes 76562976 | solution.py:97
  80.2 1.5 fusion.40
  81.8 0.9 convert_element_type.81
  82.6 1.4 fusion.38
  84.0 0.9 convert_element_type.82
  84.9 2.4 convolution_convert_fusion
  87.3 0.4 convolution_convert_fusion.1
  87.7 0.6 copy-done.10
  88.3 0.7 slice.26
  90.3 15.1 %conditional = ((f32[4,256]{1,0:T(4,128)S(1)}, f32[4,256]{1,0:T(4,128)S(1)}, f32[4,256,64]{1,2,0:T(8,128)}, f32[4,256]{1,0:T(4,128)S(1)}, f32[4,256]{1,0:T(4,128)}, /*index=5*/f32[4,256,128]{2,1,0:T(8,128)})) conditional(s32[]{:T(128)} %convert_element_type.80, (f32[4,256]{1,0:T(4,128)S(1)}, f32[4,256]{1,0:T(4,128)S(1)}, f32[4,256,64]{1,2,0:T(8,128)}, ...), branch_computations={%region_5.0_spmd, %region_6.9_spmd} | conditional | flops 961155072 | bytes 57939176 | solution.py:86
  90.4 0.9 broadcast_compare_fusion
  91.3 1.8 fusion.68
  93.1 1.3 fusion.66
  94.4 0.7 fusion.69
  95.2 1.3 fusion.67
  96.5 2.0 fusion.9
  98.6 1.3 multiply_add_fusion
  99.9 2.9 fusion.20
  102.8 2.6 fusion.23
  105.4 1.4 fusion.91
  106.8 0.6 iota.27
  108.7 1.4 fusion.91
  110.1 0.6 iota.27
  111.9 1.4 fusion.91
  113.3 0.6 iota.27
  115.2 1.9 convolution_bitcast_fusion.1
  117.2 2.5 fusion.48
  119.7 82.8 %reduce-scatter.3.cloned.1.call-done = bf16[128,2048]{1,0:T(8,128)(2,1)} async-done(((bf16[256,2048]{1,0:T(8,128)(2,1)}), bf16[128,2048]{1,0:T(8,128)(2,1)}) %reduce-scatter.3.cloned.1.call-update) | async-done | bytes 524304 | tf_op jit(solution)/shard_map/reduce_scatter | solution.py:169
  202.5 1.2 fusion.49
  203.8 1.4 fusion.53
  205.2 1.0 fusion.55
  206.3 0.5 all-gather.10.cloned.1.call-update
  206.9 0.5 all-gather.12.cloned.1.call-update
  207.4 0.5 all-gather.14.cloned.1.call-update
  208.0 0.2 reduce-scatter.5.cloned.1.call-start
  208.2 8.4 %all-gather.8.cloned.1.call-done = bf16[256,2048]{1,0:T(8,128)(2,1)} async-done(((bf16[128,2048]{1,0:T(8,128)(2,1)}), bf16[256,2048]{1,0:T(8,128)(2,1)}) %all-gather.8.cloned.1.call-update) | async-done | bytes 1048592 | tf_op jit(solution)/shard_map/all_gather | solution.py:175
  216.6 92.5 %all-gather.10.cloned.1.call-done = bf16[2048,1408]{1,0:T(8,128)(2,1)} async-done(((bf16[128,1408]{1,0:T(8,128)(2,1)}), bf16[2048,1408]{1,0:T(8,128)(2,1)}) %all-gather.10.cloned.1.call-update) | async-done | bytes 5767184 | tf_op jit(solution)/shard_map/all_gather | solution.py:177
  309.1 5.9 %fusion.70 = f32[256,1408]{1,0:T(8,128)} fusion(bf16[256,2048]{1,0:T(8,128)(2,1)} %all-gather.8.cloned.1.call-done, bf16[2048,1408]{1,0:T(8,128)(2,1)} %all-gather.10.cloned.1.call-done), kind=kOutput, calls=%fused_computation.105 | convolution fusion | flops 1476395008 | bytes 8257536 | tf_op jit(solution)/shard_map/dot_general | solution.py:181
  315.0 84.1 %all-gather.12.cloned.1.call-done = bf16[2048,1408]{1,0:T(8,128)(2,1)} async-done(((bf16[128,1408]{1,0:T(8,128)(2,1)}), bf16[2048,1408]{1,0:T(8,128)(2,1)}) %all-gather.12.cloned.1.call-update) | async-done | bytes 5767184 | tf_op jit(solution)/shard_map/all_gather | solution.py:178
  399.1 109.6 %all-gather.14.cloned.1.call-done = bf16[1408,2048]{1,0:T(8,128)(2,1)} async-done(((bf16[1408,128]{1,0:T(8,128)(2,1)}), bf16[1408,2048]{1,0:T(8,128)(2,1)}) %all-gather.14.cloned.1.call-update) | async-done | bytes 5767184 | tf_op jit(solution)/shard_map/all_gather | solution.py:179
  508.7 9.5 %convolution_convert_fusion.2 = bf16[256,2048]{1,0:T(8,128)(2,1)} fusion(bf16[1408,2048]{1,0:T(8,128)(2,1)} %all-gather.14.cloned.1.call-done, bf16[256,2048]{1,0:T(8,128)(2,1)} %all-gather.8.cloned.1.call-done, bf16[2048,1408]{1,0:T(8,128)(2,1)} %all-gather.12.cloned.1.call-done, f32[256,1408]{1,0:T(8,128)} %fusion.70), kind=kOutput, calls=%fused_computation.57 | convolution fusion | flops 2955476992 | bytes 15073280 | tf_op jit(solution)/shard_map/dot_general | solution.py:186
  518.2 6.7 %reduce-scatter.5.cloned.1.call-done = bf16[128,2048]{1,0:T(8,128)(2,1)} async-done(((bf16[256,2048]{1,0:T(8,128)(2,1)}), bf16[128,2048]{1,0:T(8,128)(2,1)}) %reduce-scatter.5.cloned.1.call-update) | async-done | bytes 524304 | tf_op jit(solution)/shard_map/reduce_scatter | solution.py:185
  525.0 2.0 fusion.56
  (56 shorter events, 0.7 us)
Async XLA Ops:
  6.5 108.7 %copy-start = (bf16[4,128,2048]{2,1,0:T(8,128)(2,1)S(1)}, bf16[4,128,2048]{2,1,0:T(8,128)(2,1)}, u32[]{:S(2)}) copy-start(bf16[4,128,2048]{2,1,0:T(8,128)(2,1)} %param.34) | copy-start | bytes 6291460
  6.5 67.7 %all-gather.6.cloned.1.call-start = ((), (), s32[]{:S(2)}) async-start(), calls=%async_computation.2 | async-start | bytes 2228224 | tf_op jit(solution)/shard_map/all_gather | solution.py:155
  9.4 193.1 %reduce-scatter.3.cloned.1.call-start = ((), (), s32[]{:S(2)}) async-start(), calls=%async_computation.3 | async-start | bytes 1572864 | tf_op jit(solution)/shard_map/reduce_scatter | solution.py:169
  80.2 4.7 copy-start.1
  81.8 5.9 %copy-start.11 = (s32[256]{0:T(256)S(1)}, s32[256]{0:T(256)}, u32[]{:S(2)}) copy-start(s32[256]{0:T(256)} %get-tuple-element.684) | copy-start | bytes 3076 | tf_op jit(solution)/shard_map/while/body/eval_jaxpr/cond
  87.7 0.6 copy-start.10
  90.3 2.7 copy-start.5
  90.3 2.7 copy-start.6
  93.1 1.3 copy-start.4
  94.4 0.8 copy-start.7
  96.5 3.4 copy-start.2
  98.6 4.2 copy-start.3
  115.2 2.0 copy-start.8
  117.1 86.6 %copy-start.9 = (bf16[128,2048]{1,0:T(8,128)(2,1)S(1)}, bf16[128,2048]{1,0:T(8,128)(2,1)}, u32[]{:S(2)}) copy-start(bf16[128,2048]{1,0:T(8,128)(2,1)} %param.23) | copy-start | bytes 1572868
  117.1 86.6 %copy-start.12 = (f32[2048]{0:T(1024)S(1)}, f32[2048]{0:T(1024)}, u32[]{:S(2)}) copy-start(f32[2048]{0:T(1024)} %param.35) | copy-start | bytes 24580
  117.2 88.1 %copy-start.13 = (f32[2048]{0:T(1024)S(1)}, f32[2048]{0:T(1024)}, u32[]{:S(2)}) copy-start(f32[2048]{0:T(1024)} %param.36) | copy-start | bytes 24580
  119.7 96.9 %all-gather.8.cloned.1.call-start = ((), (), s32[]{:S(2)}) async-start(), calls=%async_computation.4 | async-start | bytes 1572864 | tf_op jit(solution)/shard_map/all_gather | solution.py:175
  206.2 102.9 %all-gather.10.cloned.1.call-start = ((), (), s32[]{:S(2)}) async-start(), calls=%async_computation.5 | async-start | bytes 6127616 | tf_op jit(solution)/shard_map/all_gather | solution.py:177
  206.8 192.3 %all-gather.12.cloned.1.call-start = ((), (), s32[]{:S(2)}) async-start(), calls=%async_computation.6 | async-start | bytes 6127616 | tf_op jit(solution)/shard_map/all_gather | solution.py:178
  207.4 301.3 %all-gather.14.cloned.1.call-start = ((), (), s32[]{:S(2)}) async-start(), calls=%async_computation.7 | async-start | bytes 6127616 | tf_op jit(solution)/shard_map/all_gather | solution.py:179
  208.0 317.0 %reduce-scatter.5.cloned.1.call-start = ((), (), s32[]{:S(2)}) async-start(), calls=%async_computation.8 | async-start | bytes 1572864 | tf_op jit(solution)/shard_map/reduce_scatter | solution.py:185
Sparse Core Ops, SparseCore 0:
  10.1 64.0 all-gather.5
  119.8 82.6 reduce-scatter.2
  206.4 10.2 all-gather.7
  219.2 89.9 all-gather.9
  311.7 87.4 all-gather.11
  401.7 106.9 all-gather.13
  518.4 6.5 reduce-scatter.4
where the time goes:
time: 536 us; the launch traced here: 534 us
  waiting for transfers between devices  394 us (74%)
  blocking collectives  47.5 us (9%)
  matrix products  36 us (7%)
  other arithmetic  23.2 us (4%)
  between operations  13.6 us (3%)
  local copies, waits for them, and re-layouts  12.5 us (2%)
  loops' own time  6.69 us (1%)
    all_gather x1, waiting for transfers between devices, shards(): lax.all_gather(down_weight, 'sp', axis=1, tiled=True)  110 us
    all_gather x1, waiting for transfers between devices, shards(): lax.all_gather(gate_weight, 'sp', axis=0, tiled=True)  92.5 us
    all_gather x1, waiting for transfers between devices, shards(): lax.all_gather(up_weight, 'sp', axis=0, tiled=True)  84.1 us
    reduce_scatter x1, waiting for transfers between devices, shards(): lax.psum_scatter(term.astype(jnp.bfloat16), 'tp', scatter_dimension=0, ti...  82.8 us
    all_gather x1, blocking collectives, shards(): lax.all_gather(sent_rot, 'sp', axis=0, tiled=True)  47.5 us
  transfers between devices with their start and end apart: 7, of which 7 were waited for; matrix products, arithmetic and copies ran while one was open for 3% of the time, Pallas kernels for 0%

commit v1 on v0

--- a/solution.py
+++ b/solution.py
@@ -7,6 +7,11 @@
 THETA = 10000.0
 EPS = 1e-06
 NEGATIVE = -1e30
+
+
+def gathered_along(array, axis, dim):
+    pieces = lax.all_gather(array, axis)
+    return jnp.concatenate(pieces, axis=dim)
 
 
 def rotate(values, positions):
@@ -176,7 +181,7 @@
     gate_whole, up_whole, down_whole = (
         lax.all_gather(gate_weight, "sp", axis=0, tiled=True),
         lax.all_gather(up_weight, "sp", axis=0, tiled=True),
-        lax.all_gather(down_weight, "sp", axis=1, tiled=True),
+        gathered_along(down_weight, "sp", 1),
     )
     gate = jnp.dot(whole_normed, gate_whole, preferred_element_type=jnp.float32)
     up = jnp.dot(whole_normed, up_whole, preferred_element_type=jnp.float32)

time: 536 us -> 514 us (0.959)
  waiting for transfers between devices: 394 us -> 364 us
  local copies, waits for them, and re-layouts: 12.5 us -> 20.8 us
    all_gather x1, waiting for transfers between devices: 110 us -> 87.6 us  [gathered_along(): pieces = lax.all_gather(array, axis)]
    reshape x0 -> x1, local copies, waits for them, and re-layouts: none -> 8.27 us  [gathered_along(): return jnp.concatenate(pieces, axis=dim)]
    all_gather x1, waiting for transfers between devices: 8.42 us -> 0.86 us  [shards(): whole_normed = lax.all_gather(normed, 'tp', axis=0, tiled=True)]
  transfers between devices with their start and end apart: 7 -> 7, of which waited for: 7 -> 7; matrix products, arithmetic and copies ran while one was open for 3% -> 5% of each run, Pallas kernels for 0% -> 0%
where the time goes in v1:
time: 514 us; the launch traced here: 512 us
  waiting for transfers between devices  364 us (71%)
  blocking collectives  47.5 us (9%)
  matrix products  36 us (7%)
  other arithmetic  23.2 us (5%)
  local copies, waits for them, and re-layouts  20.8 us (4%)
  between operations  13.6 us (3%)
  loops' own time  6.69 us (1%)
    all_gather x1, waiting for transfers between devices, shards(): lax.all_gather(gate_weight, 'sp', axis=0, tiled=True)  92.5 us
    all_gather x1, waiting for transfers between devices, gathered_along(): pieces = lax.all_gather(array, axis)  87.6 us
    all_gather x1, waiting for transfers between devices, shards(): lax.all_gather(up_weight, 'sp', axis=0, tiled=True)  84.1 us
    reduce_scatter x1, waiting for transfers between devices, shards(): lax.psum_scatter(term.astype(jnp.bfloat16), 'tp', scatter_dimension=0, ti...  82 us
    all_gather x1, blocking collectives, shards(): lax.all_gather(sent_rot, 'sp', axis=0, tiled=True)  47.5 us
  transfers between devices with their start and end apart: 7, of which 7 were waited for; matrix products, arithmetic and copies ran while one was open for 5% of the time, Pallas kernels for 0%

profile of v1, /device:TPU:0, one launch (start us, length us, event | category | flops | bytes accessed | tf_op | source)
XLA Modules:
  0.0 512.4 jit_solution(2298064215357424612)
XLA Ops:
  6.5 1.2 fusion.57
  7.7 1.7 fusion.59
  9.5 0.7 convert_element_type.107
  10.2 0.6 slice.38
  10.8 1.0 slice.45
  11.8 0.9 copy.36
  12.7 1.0 copy.31
  13.7 1.7 copy.32
  15.4 0.9 slice.39
  16.5 0.9 slice_convert_fusion
  17.4 0.7 pad_maximum_fusion
  18.1 0.6 pad_maximum_fusion.1
  18.7 47.5 %all_gather.22 = bf16[4096,32]{0,1:T(8,128)(2,1)} all-gather(bf16[256,32]{0,1:T(8,128)(2,1)S(1)} %pad_maximum_fusion.2), channel_id=1, replica_groups=mesh['sp'=16,'tp'=2] {'sp'}, dimensions={0}, use_global_device_ids=true | all-gather | bytes 278528 | tf_op jit(solution)/shard_map/all_gather | solution.py:161
  66.2 8.1 %all-gather.7.cloned.1.call-done = bf16[4096,256]{1,0:T(8,128)(2,1)} async-done(((bf16[256,256]{1,0:T(8,128)(2,1)}), bf16[4096,256]{1,0:T(8,128)(2,1)}) %all-gather.7.cloned.1.call-update) | async-done | bytes 2097168 | tf_op jit(solution)/shard_map/all_gather | solution.py:160
  74.2 0.6 iota.15
  74.8 0.8 broadcast_in_dim.44
  75.7 0.7 broadcast_in_dim.43
  76.4 0.6 broadcast.136.clone
  77.0 38.2 %while.24 = (s32[]{:T(128)}, f32[4,256]{1,0:T(4,128)S(1)}, f32[4,256]{1,0:T(4,128)S(1)}, f32[4,256,64]{1,2,0:T(8,128)}, f32[4,256]{1,0:T(4,128)S(1)}, /*index=5*...) while((s32[]{:T(128)}, f32[4,256]{1,0:T(4,128)S(1)}, ...), condition=%wide.region_11.12_spmd.clone, body=%wide.region_1.11_spmd.clone.sunk | while | flops 1768035584 | bytes 76572688 | solution.py:104
  77.0 1.4 fusion.91
  78.4 0.6 iota.27
  80.2 25.2 %conditional.4 = ((f32[4,256]{1,0:T(4,128)S(1)}, f32[4,256]{1,0:T(4,128)S(1)}, f32[4,256,64]{1,2,0:T(8,128)}, f32[4,256]{1,0:T(4,128)S(1)}, f32[4,256]{1,0:T(4,128)}, /*index=5*/f32[4,256,128]{2,1,0:T(8,128)})) conditional(s32[]{:T(128)} %convert_element_type.184, (f32[4,256]{1,0:T(4,128)S(1)}, f32[4,256]{1,0:T(4,128)S(1)}, f32[4,256,64]{1,2,0:T(8,128)}, ...), branch_computations={%region_3.0_spmd, %region_4.10_spmd} | conditional | flops 1768034560 | bytes 76562976 | solution.py:102
  80.2 1.5 fusion.40
  81.8 0.9 convert_element_type.81
  82.6 1.4 fusion.38
  84.0 0.9 convert_element_type.82
  84.9 2.4 convolution_convert_fusion
  87.3 0.4 convolution_convert_fusion.1
  87.7 0.6 copy-done.10
  88.3 0.7 slice.26
  90.3 15.1 %conditional = ((f32[4,256]{1,0:T(4,128)S(1)}, f32[4,256]{1,0:T(4,128)S(1)}, f32[4,256,64]{1,2,0:T(8,128)}, f32[4,256]{1,0:T(4,128)S(1)}, f32[4,256]{1,0:T(4,128)}, /*index=5*/f32[4,256,128]{2,1,0:T(8,128)})) conditional(s32[]{:T(128)} %convert_element_type.80, (f32[4,256]{1,0:T(4,128)S(1)}, f32[4,256]{1,0:T(4,128)S(1)}, f32[4,256,64]{1,2,0:T(8,128)}, ...), branch_computations={%region_5.0_spmd, %region_6.9_spmd} | conditional | flops 961155072 | bytes 57939176 | solution.py:91
  90.4 0.9 broadcast_compare_fusion
  91.3 1.8 fusion.68
  93.1 1.3 fusion.66
  94.4 0.7 fusion.69
  95.2 1.3 fusion.67
  96.5 2.0 fusion.9
  98.6 1.3 multiply_add_fusion
  99.9 2.9 fusion.20
  102.8 2.6 fusion.23
  105.4 1.4 fusion.91
  106.8 0.6 iota.27
  108.7 1.4 fusion.91
  110.1 0.6 iota.27
  111.9 1.4 fusion.91
  113.3 0.6 iota.27
  115.2 1.9 convolution_bitcast_fusion.1
  117.2 2.5 fusion.48
  119.7 0.7 all-gather.15.cloned.1.call-update
  120.5 82.0 %reduce-scatter.3.cloned.1.call-done = bf16[128,2048]{1,0:T(8,128)(2,1)} async-done(((bf16[256,2048]{1,0:T(8,128)(2,1)}), bf16[128,2048]{1,0:T(8,128)(2,1)}) %reduce-scatter.3.cloned.1.call-update) | async-done | bytes 524304 | tf_op jit(solution)/shard_map/reduce_scatter | solution.py:174
  202.5 1.2 fusion.49
  203.8 1.4 fusion.53
  205.2 1.0 fusion.55
  206.3 0.5 all-gather.11.cloned.1.call-update
  206.9 0.5 all-gather.13.cloned.1.call-update
  207.6 87.6 %all-gather.15.cloned.1.call-done = bf16[22528,128]{1,0:T(8,128)(2,1)} async-done(((bf16[1408,128]{1,0:T(8,128)(2,1)}), bf16[22528,128]{1,0:T(8,128)(2,1)}) %all-gather.15.cloned.1.call-update) | async-done | bytes 5767184 | tf_op jit(solution)/shard_map/all_gather | solution.py:13
  295.2 8.3 %copy.33 = bf16[1408,16,128]{0,2,1:T(8,128)(2,1)} copy(bf16[1408,16,128]{2,0,1:T(8,128)(2,1)} %bitcast.65) | data formatting | bytes 11534336 | tf_op jit(solution)/shard_map/reshape | solution.py:14
  303.5 0.9 all-gather.9.cloned.1.call-done
  304.3 92.5 %all-gather.11.cloned.1.call-done = bf16[2048,1408]{1,0:T(8,128)(2,1)} async-done(((bf16[128,1408]{1,0:T(8,128)(2,1)}), bf16[2048,1408]{1,0:T(8,128)(2,1)}) %all-gather.11.cloned.1.call-update) | async-done | bytes 5767184 | tf_op jit(solution)/shard_map/all_gather | solution.py:182
  396.8 5.9 %fusion.70 = f32[256,1408]{1,0:T(8,128)} fusion(bf16[256,2048]{1,0:T(8,128)(2,1)} %all-gather.9.cloned.1.call-done, bf16[2048,1408]{1,0:T(8,128)(2,1)} %all-gather.11.cloned.1.call-done), kind=kOutput, calls=%fused_computation.105 | convolution fusion | flops 1476395008 | bytes 8257536 | tf_op jit(solution)/shard_map/dot_general | solution.py:186
  402.7 84.1 %all-gather.13.cloned.1.call-done = bf16[2048,1408]{1,0:T(8,128)(2,1)} async-done(((bf16[128,1408]{1,0:T(8,128)(2,1)}), bf16[2048,1408]{1,0:T(8,128)(2,1)}) %all-gather.13.cloned.1.call-update) | async-done | bytes 5767184 | tf_op jit(solution)/shard_map/all_gather | solution.py:183
  486.8 9.5 %convolution_convert_fusion.2 = bf16[256,2048]{1,0:T(8,128)(2,1)} fusion(bf16[1408,2048]{0,1:T(8,128)(2,1)} %bitcast.66, bf16[256,2048]{1,0:T(8,128)(2,1)} %all-gather.9.cloned.1.call-done, bf16[2048,1408]{1,0:T(8,128)(2,1)} %all-gather.13.cloned.1.call-done, f32[256,1408]{1,0:T(8,128)} %fusion.70), kind=kOutput, calls=%fused_computation.57 | convolution fusion | flops 2955476992 | bytes 15073280 | tf_op jit(solution)/shard_map/dot_general | solution.py:191
  496.4 7.2 %reduce-scatter.5.cloned.1.call-done = bf16[128,2048]{1,0:T(8,128)(2,1)} async-done(((bf16[256,2048]{1,0:T(8,128)(2,1)}), bf16[128,2048]{1,0:T(8,128)(2,1)}) %reduce-scatter.5.cloned.1.call-update) | async-done | bytes 524304 | tf_op jit(solution)/shard_map/reduce_scatter | solution.py:190
  503.6 2.0 fusion.56
  (57 shorter events, 1.0 us)
Async XLA Ops:
  6.5 108.7 %copy-start = (bf16[4,128,2048]{2,1,0:T(8,128)(2,1)S(1)}, bf16[4,128,2048]{2,1,0:T(8,128)(2,1)}, u32[]{:S(2)}) copy-start(bf16[4,128,2048]{2,1,0:T(8,128)(2,1)} %param.34) | copy-start | bytes 6291460
  6.5 67.7 %all-gather.7.cloned.1.call-start = ((), (), s32[]{:S(2)}) async-start(), calls=%async_computation.2 | async-start | bytes 2228224 | tf_op jit(solution)/shard_map/all_gather | solution.py:160
  9.4 193.1 %reduce-scatter.3.cloned.1.call-start = ((), (), s32[]{:S(2)}) async-start(), calls=%async_computation.3 | async-start | bytes 1572864 | tf_op jit(solution)/shard_map/reduce_scatter | solution.py:174
  80.2 4.7 copy-start.1
  81.8 5.9 %copy-start.11 = (s32[256]{0:T(256)S(1)}, s32[256]{0:T(256)}, u32[]{:S(2)}) copy-start(s32[256]{0:T(256)} %get-tuple-element.724) | copy-start | bytes 3076 | tf_op jit(solution)/shard_map/while/body/eval_jaxpr/cond
  87.7 0.6 copy-start.10
  90.3 2.7 copy-start.5
  90.3 2.7 copy-start.6
  93.1 1.3 copy-start.4
  94.4 0.8 copy-start.7
  96.5 3.4 copy-start.2
  98.6 4.2 copy-start.3
  115.2 2.0 copy-start.8
  117.1 86.6 %copy-start.9 = (bf16[128,2048]{1,0:T(8,128)(2,1)S(1)}, bf16[128,2048]{1,0:T(8,128)(2,1)}, u32[]{:S(2)}) copy-start(bf16[128,2048]{1,0:T(8,128)(2,1)} %param.23) | copy-start | bytes 1572868
  117.1 86.6 %copy-start.12 = (f32[2048]{0:T(1024)S(1)}, f32[2048]{0:T(1024)}, u32[]{:S(2)}) copy-start(f32[2048]{0:T(1024)} %param.35) | copy-start | bytes 24580
  117.2 88.1 %copy-start.13 = (f32[2048]{0:T(1024)S(1)}, f32[2048]{0:T(1024)}, u32[]{:S(2)}) copy-start(f32[2048]{0:T(1024)} %param.36) | copy-start | bytes 24580
  119.7 175.5 %all-gather.15.cloned.1.call-start = ((), (), s32[]{:S(2)}) async-start(), calls=%async_computation.8 | async-start | bytes 6127616 | tf_op jit(solution)/shard_map/all_gather | solution.py:13
  120.4 183.9 %all-gather.9.cloned.1.call-start = ((), (), s32[]{:S(2)}) async-start(), calls=%async_computation.4 | async-start | bytes 1572864 | tf_op jit(solution)/shard_map/all_gather | solution.py:180
  206.2 190.6 %all-gather.11.cloned.1.call-start = ((), (), s32[]{:S(2)}) async-start(), calls=%async_computation.5 | async-start | bytes 6127616 | tf_op jit(solution)/shard_map/all_gather | solution.py:182
  206.8 280.0 %all-gather.13.cloned.1.call-start = ((), (), s32[]{:S(2)}) async-start(), calls=%async_computation.6 | async-start | bytes 6127616 | tf_op jit(solution)/shard_map/all_gather | solution.py:183
  207.4 296.2 %reduce-scatter.5.cloned.1.call-start = ((), (), s32[]{:S(2)}) async-start(), calls=%async_computation.7 | async-start | bytes 1572864 | tf_op jit(solution)/shard_map/reduce_scatter | solution.py:190
Sparse Core Ops, SparseCore 0:
  10.1 64.0 all-gather.6
  119.8 82.6 reduce-scatter.2
  205.2 89.9 all-gather.14
  296.6 7.6 all-gather.8
  306.9 89.9 all-gather.10
  399.4 87.4 all-gather.12
  496.5 7.0 reduce-scatter.4
